TPU v7x, 32 devices: a whole 2x2x4 slice. The times are simulated.
32 devices in a mesh: sp: 16 (over z, y, core), tp: 2 (over x).
Axes of the slice: x: 2, y: 2, z: 4, core: 2. Of those that a mesh axis runs over, the one named last changes fastest.
Arguments:
- tokens: bfloat16 [1024, 4, 2048], P(('sp', 'tp')), may hold values from -16 to 16
- norm_gain: float32 [2048], replicated, may hold values from 0.1 to 1.9
- w_query: bfloat16 [2048, 2048], P('sp', 'tp'), may hold values from -0.125 to 0.125
- w_forget: bfloat16 [2048, 2048], P('sp', 'tp'), may hold values from -0.125 to 0.125
- w_value: bfloat16 [2048, 2048], P('sp', 'tp'), may hold values from -0.125 to 0.125
- floor_gap: float32 [2048], P('tp'), may hold values from 0 to 0.15, as said below
- head_gain: float32 [2048], P('tp'), may hold values from 0.1 to 1.9
- w_out: bfloat16 [2048, 2048], P('tp', 'sp'), may hold values from -0.125 to 0.125
Outputs:
- mixed: bfloat16 [1024, 4, 2048], P(('sp', 'tp'))
Inputs may be any that keep to these rules, and one draw needn't show every extreme that they name: `floor_gap`: positive, at least 0.5 / 1024 and at most 0.15.
All inputs are finite; a program needn't handle non-finite values.
Results may differ from a plain program's by a relative error of at most 0.014.
Values may be sent and summed in bfloat16 or wider, within the bound.
A program may use at most 128 MiB of HBM per device.

v0:
```python
import math
import jax
import jax.numpy as jnp
from jax import lax
from jax.sharding import PartitionSpec as P

KEY_DIM = 128
VAL_DIM = 128
eps_norm = 1e-06
highest = lax.Precision.HIGHEST


def carried_in(value, axis, combine, identity):
    length, mine = (lax.axis_size(axis), lax.axis_index(axis))
    everything = jax.tree.map(lambda part: lax.all_gather(part, axis), value)
    start = jax.tree.map(
        lambda part, zero: jnp.broadcast_to(jnp.asarray(zero, part.dtype), part.shape),
        value,
        identity,
    )

    def hop(k, before):
        reached = k < mine
        new = combine(before, jax.tree.map(lambda part: part[k], everything))
        return jax.tree.map(lambda a, b: jnp.where(reached, a, b), new, before)

    return lax.fori_loop(0, length, hop, start)


def link_states(earlier, later):
    decay_early, state_early = earlier
    decay_late, state_late = later
    return (decay_early * decay_late, decay_late[..., None] * state_early + state_late)


def local_pass(query, inkey, log_forget, values):
    block_len = query.shape[1]
    cumulative = jnp.cumsum(log_forget, axis=1)
    final = cumulative[:, -1]
    query_scaled = query * jnp.exp(cumulative)
    key_scaled = inkey * jnp.exp(-cumulative)
    key_final = inkey * jnp.exp(final[:, None] - cumulative)
    scores = jnp.einsum("ntshk,nushk->nshtu", query_scaled, key_scaled, precision=highest)
    positions = lax.iota(jnp.int32, block_len)
    causal = positions[:, None] >= positions[None, :]
    scores = jnp.where(causal, scores, 0.0)
    inside = jnp.einsum("nshtu,nushv->ntshv", scores, values, precision=highest)
    updates = jnp.einsum("nushk,nushv->nshkv", key_final, values, precision=highest)
    block_decay = jnp.exp(final)

    def advance(carry, inputs):
        decay_block, update_block = inputs
        return (decay_block[..., None] * carry + update_block, carry)

    end_state, entering = lax.scan(advance, jnp.zeros_like(updates[0]), (block_decay, updates))
    inside = inside + jnp.einsum("ntshk,nshkv->ntshv", query_scaled, entering, precision=highest)
    offsets = jnp.cumsum(final, axis=0) - final
    reach = query_scaled * jnp.exp(offsets)[:, None]
    total_decay = jnp.exp(jnp.sum(final, axis=0))
    return (inside, reach, total_decay, end_state)


def read_out(reach, incoming):
    return jnp.einsum("ntshk,shkv->ntshv", reach, incoming, precision=highest)


def body(tokens, norm_gain, w_query, w_forget, w_value, floor_gap, head_gain, w_out):
    flat = tokens.astype(jnp.float32)
    scale = lax.rsqrt(jnp.mean(flat * flat, axis=-1, keepdims=True) + eps_norm)
    normed = (flat * scale * norm_gain).astype(jnp.bfloat16)
    whole_query, whole_forget, whole_value = (
        lax.all_gather(w_query, "sp", axis=0, tiled=True),
        lax.all_gather(w_forget, "sp", axis=0, tiled=True),
        lax.all_gather(w_value, "sp", axis=0, tiled=True),
    )
    key_width = whole_query.shape[1]
    piece = lax.all_gather(normed, "tp", axis=0, tiled=True)
    flat_rows = piece.reshape(-1, piece.shape[-1])
    outputs = [
        jnp.dot(flat_rows, weight, preferred_element_type=jnp.float32).astype(jnp.bfloat16)
        for weight in (whole_query, whole_forget, whole_value)
    ]
    joined = jnp.concatenate(outputs, axis=1)
    projected = joined.reshape(piece.shape[0], piece.shape[1], joined.shape[1])
    projected = lax.optimization_barrier(projected).astype(jnp.float32)
    positions_dev, sequences = (projected.shape[0], projected.shape[1])
    head_count = key_width // KEY_DIM
    block_len = math.gcd(positions_dev, 128)
    block_count = positions_dev // block_len

    def blocks(value, channels):
        return value.reshape(block_count, block_len, sequences, head_count, channels)

    query = jax.nn.silu(blocks(projected[..., :key_width], KEY_DIM))
    inkey = floor_gap.reshape(head_count, KEY_DIM) * jax.nn.sigmoid(
        -blocks(projected[..., key_width : 2 * key_width], KEY_DIM)
    )
    log_forget = jnp.log1p(-inkey)
    values = blocks(projected[..., 2 * key_width :], VAL_DIM)
    inside, reach, total_decay, end_state = local_pass(query, inkey, log_forget, values)
    _, incoming = carried_in(
        (total_decay, end_state),
        "sp",
        link_states,
        (jnp.ones_like(total_decay), jnp.zeros_like(end_state)),
    )
    recurrent = inside + read_out(reach, incoming)
    mean_square = jnp.mean(recurrent * recurrent, axis=-1, keepdims=True)
    hidden = recurrent * lax.rsqrt(mean_square + eps_norm) * head_gain.reshape(head_count, VAL_DIM)
    hidden = hidden.astype(jnp.bfloat16).reshape(positions_dev, sequences, head_count * VAL_DIM)
    out_columns = lax.all_gather(w_out, "sp", axis=1, tiled=True)
    piece = hidden
    return lax.psum_scatter(
        jnp.einsum("psh,hd->psd", piece, out_columns, preferred_element_type=jnp.float32).astype(
            jnp.bfloat16
        ),
        "tp",
        scatter_dimension=0,
        tiled=True,
    )


def solution(mesh):
    return jax.shard_map(
        body,
        mesh=mesh,
        in_specs=(
            P(("sp", "tp"), None, None),
            P(),
            P("sp", "tp"),
            P("sp", "tp"),
            P("sp", "tp"),
            P("tp"),
            P("tp"),
            P("tp", "sp"),
        ),
        out_specs=P(("sp", "tp"), None, None),
        check_vma=False,
    )
```

profile of v0, /device:TPU:0, one launch (start us, length us, event | category | flops | bytes accessed | tf_op | source)
XLA Modules:
  0.0 463.9 jit_solution(16212869938098595885)
XLA Ops:
  7.9 2.2 fusion.10
  12.3 22.0 %all-gather.9.cloned.1.call-done = bf16[64,4,2048]{2,1,0:T(4,128)(2,1)} async-done(((bf16[32,4,2048]{2,1,0:T(4,128)(2,1)}), bf16[64,4,2048]{2,1,0:T(4,128)(2,1)}) %all-gather.9.cloned.1.call-update) | async-done | bytes 1048592 | tf_op jit(solution)/shard_map/all_gather | solution.py:77
  35.6 51.2 %all-gather.15.cloned.1.call-done = bf16[2048,1024]{1,0:T(8,128)(2,1)} async-done(((bf16[128,1024]{1,0:T(8,128)(2,1)}), bf16[2048,1024]{1,0:T(8,128)(2,1)}) %all-gather.15.cloned.1.call-update) | async-done | bytes 4194320 | tf_op jit(solution)/shard_map/all_gather | solution.py:74
  86.9 3.4 convolution_convert_fusion
  90.3 47.7 %all-gather.13.cloned.1.call-done = bf16[2048,1024]{1,0:T(8,128)(2,1)} async-done(((bf16[128,1024]{1,0:T(8,128)(2,1)}), bf16[2048,1024]{1,0:T(8,128)(2,1)}) %all-gather.13.cloned.1.call-update) | async-done | bytes 4194320 | tf_op jit(solution)/shard_map/all_gather | solution.py:73
  138.0 4.2 convolution_convert_fusion.1
  142.2 46.7 %all-gather.11.cloned.1.call-done = bf16[2048,1024]{1,0:T(8,128)(2,1)} async-done(((bf16[128,1024]{1,0:T(8,128)(2,1)}), bf16[2048,1024]{1,0:T(8,128)(2,1)}) %all-gather.11.cloned.1.call-update) | async-done | bytes 4194320 | tf_op jit(solution)/shard_map/all_gather | solution.py:72
  188.9 3.5 convolution_convert_fusion.2
  200.4 3.8 fusion.17
  204.2 3.7 convolution_add_fusion
  208.8 4.1 convolution_select_fusion
  213.7 2.5 fusion.6
  216.2 21.5 %all-gather = f32[16,1,4,8,128]{4,3,2,1,0:T(8,128)S(1)} all-gather(f32[1,1,4,8,128]{4,3,2,1,0:T(8,128)S(1)} %get-tuple-element.151), channel_id=2, replica_groups=mesh['sp'=16,'tp'=2] {'sp'}, dimensions={0}, use_global_device_ids=true | all-gather | bytes 278528 | tf_op jit(solution)/shard_map/all_gather | solution.py:15
  237.7 139.0 %all-gather.19.cloned.1.call-done = f32[64,8,128,128]{3,2,1,0:T(8,128)} async-done(((f32[4,8,128,128]{3,2,1,0:T(8,128)}), f32[64,8,128,128]{3,2,1,0:T(8,128)}) %all-gather.19.cloned.1.call-update) | async-done | bytes 33554448 | tf_op jit(solution)/shard_map/all_gather | solution.py:15
  376.7 35.5 %while.9 = (s32[]{:T(128)}, f32[4,8,128,128]{3,2,1,0:T(8,128)S(1)}, s32[]{:T(128)}, f32[16,4,8,128]{3,2,1,0:T(8,128)S(1)}, f32[16,4,8,128,128]{4,3,2,1,0:T(8,128)}, /*index=5*/s32[]{:T(128)}, s32[]{:T(128)}) while((s32[]{:T(128)}, f32[4,8,128,128]{3,2,1,0:T(8,128)S(1)}, s32[]{:T(128)}, f32[16,4,8,128]{3,2,1,0:T(8,128)S(1)}, ...), condition=%wide.region_3.4_spmd.clone, body=%wide.region_2.3_spmd.clone.sunk | while | flops 2097156 | bytes 6340721 | solution.py:27
  376.7 2.2 fusion.44
  379.0 2.2 fusion.44
  381.2 2.2 fusion.44
  383.5 2.2 fusion.44
  385.7 2.2 fusion.44
  387.9 2.2 fusion.44
  390.1 2.2 fusion.44
  392.3 2.2 fusion.44
  394.6 2.2 fusion.44
  399.0 2.2 fusion.44
  405.6 2.2 fusion.44
  407.8 2.2 fusion.44
  412.3 3.8 multiply_reduce_fusion
  417.0 14.6 %all-gather.17.cloned.1.call-done = bf16[1024,2048]{1,0:T(8,128)(2,1)} async-done(((bf16[1024,128]{1,0:T(8,128)(2,1)}), bf16[1024,2048]{1,0:T(8,128)(2,1)}) %all-gather.17.cloned.1.call-update) | async-done | bytes 4194320 | tf_op jit(solution)/shard_map/all_gather | solution.py:111
  431.6 4.4 fusion.3
  436.1 18.7 %reduce-scatter.2.cloned.1.call-done = bf16[32,4,2048]{2,0,1:T(8,128)(2,1)} async-done(((bf16[64,4,2048]{2,0,1:T(8,128)(2,1)}), bf16[32,4,2048]{2,0,1:T(8,128)(2,1)}) %reduce-scatter.2.cloned.1.call-update) | async-done | bytes 524304 | tf_op jit(solution)/shard_map/reduce_scatter | solution.py:113
  454.8 2.2 copy.30
  (74 shorter events, 24.0 us)
Async XLA Ops:
  6.5 27.8 %all-gather.9.cloned.1.call-start = ((), (), s32[]{:S(2)}) async-start(), calls=%async_computation.1 | async-start | bytes 1572864 | tf_op jit(solution)/shard_map/all_gather | solution.py:77
  10.1 76.7 %all-gather.15.cloned.1.call-start = ((), (), s32[]{:S(2)}) async-start(), calls=%async_computation.4 | async-start | bytes 4456448 | tf_op jit(solution)/shard_map/all_gather | solution.py:74
  10.9 127.1 %all-gather.13.cloned.1.call-start = ((), (), s32[]{:S(2)}) async-start(), calls=%async_computation.3 | async-start | bytes 4456448 | tf_op jit(solution)/shard_map/all_gather | solution.py:73
  11.6 177.3 %all-gather.11.cloned.1.call-start = ((), (), s32[]{:S(2)}) async-start(), calls=%async_computation.2 | async-start | bytes 4456448 | tf_op jit(solution)/shard_map/all_gather | solution.py:72
  12.2 364.5 %all-gather.19.cloned.1.call-start = ((), (), s32[]{:S(2)}) async-start(), calls=%async_computation.7 | async-start | bytes 35651584 | tf_op jit(solution)/shard_map/all_gather | solution.py:15
  188.9 3.5 copy-start.5
  193.2 3.9 copy-start
  197.0 1.2 copy-start.4
  197.0 1.2 copy-start.6
  198.2 2.0 slice-start
  200.4 3.8 copy-start.1
  207.9 223.7 %all-gather.17.cloned.1.call-start = ((), (), s32[]{:S(2)}) async-start(), calls=%async_computation.5 | async-start | bytes 4456448 | tf_op jit(solution)/shard_map/all_gather | solution.py:111
  208.5 246.3 %reduce-scatter.2.cloned.1.call-start = ((), (), s32[]{:S(2)}) async-start(), calls=%async_computation.6 | async-start | bytes 1572864 | tf_op jit(solution)/shard_map/reduce_scatter | solution.py:113
  208.8 4.1 copy-start.2
  376.7 35.5 %copy-start.3 = (f32[64,4,8,128]{3,2,1,0:T(8,128)S(1)}, f32[64,4,8,128]{3,2,1,0:T(8,128)}, u32[]{:S(2)}) copy-start(f32[64,4,8,128]{3,2,1,0:T(8,128)} %get-tuple-element.147) | copy-start | bytes 3145732
  412.3 3.8 copy-start.7
Sparse Core Ops, SparseCore 0:
  10.3 23.9 all-gather.8
  36.5 50.3 all-gather.14
  89.0 48.8 all-gather.12
  140.0 48.8 all-gather.10
  208.1 168.6 all-gather.18
  378.7 52.8 all-gather.16
  436.2 18.5 reduce-scatter.1
where the time goes:
time: 465 us; the launch traced here: 464 us
  waiting for transfers between devices  343 us (74%)
  other arithmetic  44.1 us (9%)
  matrix products  30.4 us (7%)
  blocking collectives  21.5 us (5%)
  between operations  13.7 us (3%)
  local copies, waits for them, and re-layouts  10.6 us (2%)
    all_gather x1, waiting for transfers between devices, carried_in(): everything = jax.tree.map(lambda part: lax.all_gather(part, axis), value)  139 us
    all_gather x1, waiting for transfers between devices, body(): lax.all_gather(w_value, 'sp', axis=0, tiled=True)  51.2 us
    all_gather x1, waiting for transfers between devices, body(): lax.all_gather(w_forget, 'sp', axis=0, tiled=True)  47.7 us
    all_gather x1, waiting for transfers between devices, body(): lax.all_gather(w_query, 'sp', axis=0, tiled=True)  46.7 us
    select_n x16, other arithmetic, hop(): return jax.tree.map(lambda a, b: jnp.where(reached, a, b), new, before)  34.8 us
    all_gather x1, waiting for transfers between devices, body(): piece = lax.all_gather(normed, 'tp', axis=0, tiled=True)  22 us
    all_gather x1, blocking collectives, carried_in(): everything = jax.tree.map(lambda part: lax.all_gather(part, axis), value)  21.5 us
    reduce_scatter x1, waiting for transfers between devices, body(): lax.psum_scatter(jnp.einsum('psh,hd->psd', piece, out_columns, preferred_...  18.7 us
  transfers between devices with their start and end apart: 7, of which 7 were waited for; matrix products, arithmetic and copies ran while one was open for 12% of the time, Pallas kernels for 0%

commit v1 on v0

--- a/solution.py
+++ b/solution.py
@@ -8,6 +8,19 @@
 VAL_DIM = 128
 eps_norm = 1e-06
 highest = lax.Precision.HIGHEST
+
+
+def ring_gather(shard, axis, dim):
+    ways = lax.axis_size(axis)
+    up = [(d, (d + 1) % ways) for d in range(ways)]
+    down = [(d, (d - 1) % ways) for d in range(ways)]
+    earlier, later = ([shard], [shard])
+    for _ in range(ways // 2):
+        earlier.append(lax.ppermute(earlier[-1], axis, up))
+    for _ in range((ways - 1) // 2):
+        later.append(lax.ppermute(later[-1], axis, down))
+    line = jnp.concatenate([*earlier[::-1], *later[1:]], axis=dim)
+    return jnp.roll(line, (lax.axis_index(axis) - ways // 2) * shard.shape[dim], axis=dim)
 
 
 def carried_in(value, axis, combine, identity):
@@ -71,7 +84,7 @@
     whole_query, whole_forget, whole_value = (
         lax.all_gather(w_query, "sp", axis=0, tiled=True),
         lax.all_gather(w_forget, "sp", axis=0, tiled=True),
-        lax.all_gather(w_value, "sp", axis=0, tiled=True),
+        ring_gather(w_value, "sp", 0),
     )
     key_width = whole_query.shape[1]
     piece = lax.all_gather(normed, "tp", axis=0, tiled=True)

time: 465 us -> 428 us (0.920)
  waiting for transfers between devices: 343 us -> 262 us
  starting transfers between devices: 0.42 us -> 33.3 us
  local copies, waits for them, and re-layouts: 10.6 us -> 19.8 us
    all_gather x1 -> x0, waiting for transfers between devices: 51.2 us -> none  [body(): lax.all_gather(w_value, 'sp', axis=0, tiled=True)]
    all_gather x1, waiting for transfers between devices: 47.7 us -> 0.02 us  [body(): lax.all_gather(w_forget, 'sp', axis=0, tiled=True)]
    ppermute x0 -> x15, waiting for transfers between devices: none -> 43.4 us  [the longest x8 30.5 us: ring_gather(): earlier.append(lax.ppermute(earlier[-1], axis, up))]
    ppermute x0 -> x15, starting transfers between devices: none -> 32.9 us  [the longest x7 32.4 us: ring_gather(): later.append(lax.ppermute(later[-1], axis, down))]
    all_gather x1, waiting for transfers between devices: 22 us -> 0.01 us  [body(): piece = lax.all_gather(normed, 'tp', axis=0, tiled=True)]
    unnamed x16 -> x49, local copies, waits for them, and re-layouts: 1.11 us -> 10.2 us
  transfers between devices with their start and end apart: 7 -> 21, of which waited for: 7 -> 16; matrix products, arithmetic and copies ran while one was open for 12% -> 15% of each run, Pallas kernels for 0% -> 0%
where the time goes in v1:
time: 428 us; the launch traced here: 427 us
  waiting for transfers between devices  262 us (61%)
  other arithmetic  46.3 us (11%)
  starting transfers between devices  33.3 us (8%)
  matrix products  29.4 us (7%)
  blocking collectives  21.4 us (5%)
  local copies, waits for them, and re-layouts  19.8 us (5%)
  between operations  14 us (3%)
    all_gather x1, waiting for transfers between devices, carried_in(): everything = jax.tree.map(lambda part: lax.all_gather(part, axis), value)  138 us
    all_gather x1, waiting for transfers between devices, body(): lax.all_gather(w_query, 'sp', axis=0, tiled=True)  45.4 us
    select_n x16, other arithmetic, hop(): return jax.tree.map(lambda a, b: jnp.where(reached, a, b), new, before)  34.8 us
    ppermute x7, starting transfers between devices, ring_gather(): later.append(lax.ppermute(later[-1], axis, down))  32.4 us
    ppermute x8, waiting for transfers between devices, ring_gather(): earlier.append(lax.ppermute(earlier[-1], axis, up))  30.5 us
    all_gather x1, blocking collectives, carried_in(): everything = jax.tree.map(lambda part: lax.all_gather(part, axis), value)  21.4 us
    reduce_scatter x1, waiting for transfers between devices, body(): lax.psum_scatter(jnp.einsum('psh,hd->psd', piece, out_columns, preferred_...  18.7 us
    all_gather x1, waiting for transfers between devices, body(): out_columns = lax.all_gather(w_out, 'sp', axis=1, tiled=True)  14.6 us
  transfers between devices with their start and end apart: 21, of which 16 were waited for; matrix products, arithmetic and copies ran while one was open for 15% of the time, Pallas kernels for 0%

profile of v1, /device:TPU:0, one launch (start us, length us, event | category | flops | bytes accessed | tf_op | source)
XLA Modules:
  0.0 426.9 jit_solution(6281294413000104947)
XLA Ops:
  12.3 9.2 %collective-permute-done = bf16[128,1024]{1,0:T(8,128)(2,1)S(1)} collective-permute-done((bf16[128,1024]{1,0:T(8,128)(2,1)}, bf16[128,1024]{1,0:T(8,128)(2,1)S(1)}, u32[]{:S(2)}, u32[]{:S(2)}) %collective-permute-start) | collective-permute-done | bytes 262176 | tf_op jit(solution)/shard_map/ppermute | solution.py:19
  21.5 4.4 %collective-permute-start.8 = (bf16[128,1024]{1,0:T(8,128)(2,1)}, bf16[128,1024]{1,0:T(8,128)(2,1)S(1)}, u32[]{:S(2)}, u32[]{:S(2)}) collective-permute-start(bf16[128,1024]{1,0:T(8,128)(2,1)} %param.14), channel_id=1, source_target_pairs={{0,30},{2,0},{4,2},{6,4},{8,6},{10,8},{12,10},{14,12},{16,14},{18,... | collective-permute-start | bytes 786440 | tf_op jit(solution)/shard_map/ppermute | solution.py:21
  26.0 4.1 collective-permute-done.1
  30.2 4.6 %collective-permute-start.9 = (bf16[128,1024]{1,0:T(8,128)(2,1)S(1)}, bf16[128,1024]{1,0:T(8,128)(2,1)S(1)}, u32[]{:S(2)}, u32[]{:S(2)}) collective-permute-start(bf16[128,1024]{1,0:T(8,128)(2,1)S(1)} %collective-permute-done.8), channel_id=1, source_target_pairs={{0,30},{2,0},{4,2},{6,4},{8,6},{10,8},{12,10},{14,12},{16,14},{18,... | collective-permute-start | bytes 786440 | tf_op jit(solution)/shard_map/ppermute | solution.py:21
  34.8 3.8 collective-permute-done.2
  38.7 4.7 %collective-permute-start.10 = (bf16[128,1024]{1,0:T(8,128)(2,1)S(1)}, bf16[128,1024]{1,0:T(8,128)(2,1)S(1)}, u32[]{:S(2)}, u32[]{:S(2)}) collective-permute-start(bf16[128,1024]{1,0:T(8,128)(2,1)S(1)} %collective-permute-done.9), channel_id=1, source_target_pairs={{0,30},{2,0},{4,2},{6,4},{8,6},{10,8},{12,10},{14,12},{16,14},{18,... | collective-permute-start | bytes 786440 | tf_op jit(solution)/shard_map/ppermute | solution.py:21
  43.4 3.8 collective-permute-done.3
  47.2 3.9 collective-permute-done.10
  51.1 4.6 %collective-permute-start.11 = (bf16[128,1024]{1,0:T(8,128)(2,1)S(1)}, bf16[128,1024]{1,0:T(8,128)(2,1)S(1)}, u32[]{:S(2)}, u32[]{:S(2)}) collective-permute-start(bf16[128,1024]{1,0:T(8,128)(2,1)S(1)} %collective-permute-done.10), channel_id=1, source_target_pairs={{0,30},{2,0},{4,2},{6,4},{8,6},{10,8},{12,10},{14,12},{16,14},{18,... | collective-permute-start | bytes 786440 | tf_op jit(solution)/shard_map/ppermute | solution.py:21
  57.6 2.4 collective-permute-done.11
  60.0 4.6 %collective-permute-start.12 = (bf16[128,1024]{1,0:T(8,128)(2,1)S(1)}, bf16[128,1024]{1,0:T(8,128)(2,1)}, u32[]{:S(2)}, u32[]{:S(2)}) collective-permute-start(bf16[128,1024]{1,0:T(8,128)(2,1)S(1)} %collective-permute-done.11), channel_id=1, source_target_pairs={{0,30},{2,0},{4,2},{6,4},{8,6},{10,8},{12,10},{14,12},{16,14},{18,... | collective-permute-start | bytes 786440 | tf_op jit(solution)/shard_map/ppermute | solution.py:21
  66.2 6.4 %collective-permute-done.12 = bf16[128,1024]{1,0:T(8,128)(2,1)} collective-permute-done((bf16[128,1024]{1,0:T(8,128)(2,1)S(1)}, bf16[128,1024]{1,0:T(8,128)(2,1)}, u32[]{:S(2)}, u32[]{:S(2)}) %collective-permute-start.12) | collective-permute-done | bytes 262176 | tf_op jit(solution)/shard_map/ppermute | solution.py:21
  72.5 4.7 %collective-permute-start.13 = (bf16[128,1024]{1,0:T(8,128)(2,1)}, bf16[128,1024]{1,0:T(8,128)(2,1)}, u32[]{:S(2)}, u32[]{:S(2)}) collective-permute-start(bf16[128,1024]{1,0:T(8,128)(2,1)} %collective-permute-done.12), channel_id=1, source_target_pairs={{0,30},{2,0},{4,2},{6,4},{8,6},{10,8},{12,10},{14,12},{16,14},{18,... | collective-permute-start | bytes 786440 | tf_op jit(solution)/shard_map/ppermute | solution.py:21
  77.2 3.0 collective-permute-done.6
  81.6 4.7 %collective-permute-start.14 = (bf16[128,1024]{1,0:T(8,128)(2,1)}, bf16[128,1024]{1,0:T(8,128)(2,1)S(1)}, u32[]{:S(2)}, u32[]{:S(2)}) collective-permute-start(bf16[128,1024]{1,0:T(8,128)(2,1)} %collective-permute-done.13), channel_id=1, source_target_pairs={{0,30},{2,0},{4,2},{6,4},{8,6},{10,8},{12,10},{14,12},{16,14},{18,... | collective-permute-start | bytes 786440 | tf_op jit(solution)/shard_map/ppermute | solution.py:21
  86.3 3.1 collective-permute-done.7
  101.1 4.2 convolution_convert_fusion
  105.4 45.4 %all-gather.10.cloned.1.call-done = bf16[2048,1024]{1,0:T(8,128)(2,1)} async-done(((bf16[128,1024]{1,0:T(8,128)(2,1)}), bf16[2048,1024]{1,0:T(8,128)(2,1)}) %all-gather.10.cloned.1.call-update) | async-done | bytes 4194320 | tf_op jit(solution)/shard_map/all_gather | solution.py:85
  150.7 3.4 convolution_convert_fusion.1
  163.4 3.8 fusion.22
  167.2 3.7 convolution_add_fusion
  171.9 4.1 convolution_select_fusion
  177.9 2.5 fusion.8
  180.3 21.4 %all-gather = f32[16,1,4,8,128]{4,3,2,1,0:T(8,128)S(1)} all-gather(f32[1,1,4,8,128]{4,3,2,1,0:T(8,128)S(1)} %get-tuple-element.151), channel_id=2, replica_groups=mesh['sp'=16,'tp'=2] {'sp'}, dimensions={0}, use_global_device_ids=true | all-gather | bytes 278528 | tf_op jit(solution)/shard_map/all_gather | solution.py:28
  201.7 138.0 %all-gather.16.cloned.1.call-done = f32[64,8,128,128]{3,2,1,0:T(8,128)} async-done(((f32[4,8,128,128]{3,2,1,0:T(8,128)}), f32[64,8,128,128]{3,2,1,0:T(8,128)}) %all-gather.16.cloned.1.call-update) | async-done | bytes 33554448 | tf_op jit(solution)/shard_map/all_gather | solution.py:28
  339.8 35.5 %while.9 = (s32[]{:T(128)}, f32[4,8,128,128]{3,2,1,0:T(8,128)S(1)}, s32[]{:T(128)}, f32[16,4,8,128]{3,2,1,0:T(8,128)S(1)}, f32[16,4,8,128,128]{4,3,2,1,0:T(8,128)}, /*index=5*/s32[]{:T(128)}, s32[]{:T(128)}) while((s32[]{:T(128)}, f32[4,8,128,128]{3,2,1,0:T(8,128)S(1)}, s32[]{:T(128)}, f32[16,4,8,128]{3,2,1,0:T(8,128)S(1)}, ...), condition=%wide.region_3.4_spmd.clone, body=%wide.region_2.3_spmd.clone.sunk | while | flops 2097156 | bytes 6340721 | solution.py:40
  339.8 2.2 fusion.49
  375.3 3.8 multiply_reduce_fusion
  380.0 14.6 %all-gather.14.cloned.1.call-done = bf16[1024,2048]{1,0:T(8,128)(2,1)} async-done(((bf16[1024,128]{1,0:T(8,128)(2,1)}), bf16[1024,2048]{1,0:T(8,128)(2,1)}) %all-gather.14.cloned.1.call-update) | async-done | bytes 4194320 | tf_op jit(solution)/shard_map/all_gather | solution.py:124
  394.6 4.4 %fusion.5 = bf16[64,4,2048]{2,0,1:T(8,128)(2,1)} fusion(bf16[64,4,1024]{2,0,1:T(8,128)(2,1)S(1)} %reshape.183, bf16[1024,2048]{1,0:T(8,128)(2,1)} %all-gather.14.cloned.1.call-done), kind=kOutput, calls=%fused_computation.7 | convolution fusion | flops 1074266112 | bytes 5767168 | tf_op jit(solution)/shard_map/psh,hd->psd/dot_general | solution.py:127
  399.1 18.7 %reduce-scatter.2.cloned.1.call-done = bf16[32,4,2048]{2,0,1:T(8,128)(2,1)} async-done(((bf16[64,4,2048]{2,0,1:T(8,128)(2,1)}), bf16[32,4,2048]{2,0,1:T(8,128)(2,1)}) %reduce-scatter.2.cloned.1.call-update) | async-done | bytes 524304 | tf_op jit(solution)/shard_map/reduce_scatter | solution.py:126
  417.8 2.2 copy.30
  (134 shorter events, 67.7 us)
Async XLA Ops:
  6.5 86.9 %copy-start.2 = (bf16[128,1024]{1,0:T(8,128)(2,1)S(1)}, bf16[128,1024]{1,0:T(8,128)(2,1)}, u32[]{:S(2)}) copy-start(bf16[128,1024]{1,0:T(8,128)(2,1)} %param.14) | copy-start | bytes 786436
  6.5 73.7 %all-gather.8.cloned.1.call-start = ((), (), s32[]{:S(2)}) async-start(), calls=%async_computation.1 | async-start | bytes 1572864 | tf_op jit(solution)/shard_map/all_gather | solution.py:90
  10.2 90.9 %all-gather.12.cloned.1.call-start = ((), (), s32[]{:S(2)}) async-start(), calls=%async_computation.3 | async-start | bytes 4456448 | tf_op jit(solution)/shard_map/all_gather | solution.py:86
  10.9 139.8 %all-gather.10.cloned.1.call-start = ((), (), s32[]{:S(2)}) async-start(), calls=%async_computation.2 | async-start | bytes 4456448 | tf_op jit(solution)/shard_map/all_gather | solution.py:85
  11.7 328.1 %all-gather.16.cloned.1.call-start = ((), (), s32[]{:S(2)}) async-start(), calls=%async_computation.6 | async-start | bytes 35651584 | tf_op jit(solution)/shard_map/all_gather | solution.py:28
  11.7 9.8 %collective-permute-start = (bf16[128,1024]{1,0:T(8,128)(2,1)}, bf16[128,1024]{1,0:T(8,128)(2,1)S(1)}, u32[]{:S(2)}, u32[]{:S(2)}) collective-permute-start(bf16[128,1024]{1,0:T(8,128)(2,1)} %param.14), channel_id=1, source_target_pairs={{0,2},{2,4},{4,6},{6,8},{8,10},{10,12},{12,14},{14,16},{16,18},{18... | collective-permute-start | bytes 786440 | tf_op jit(solution)/shard_map/ppermute | solution.py:19
  21.5 8.5 %collective-permute-start.1 = (bf16[128,1024]{1,0:T(8,128)(2,1)S(1)}, bf16[128,1024]{1,0:T(8,128)(2,1)S(1)}, u32[]{:S(2)}, u32[]{:S(2)}) collective-permute-start(bf16[128,1024]{1,0:T(8,128)(2,1)S(1)} %collective-permute-done), channel_id=1, source_target_pairs={{0,2},{2,4},{4,6},{6,8},{8,10},{10,12},{12,14},{14,16},{16,18},{18... | collective-permute-start | bytes 786440 | tf_op jit(solution)/shard_map/ppermute | solution.py:19
  21.5 8.6 %collective-permute-start.8 = (bf16[128,1024]{1,0:T(8,128)(2,1)}, bf16[128,1024]{1,0:T(8,128)(2,1)S(1)}, u32[]{:S(2)}, u32[]{:S(2)}) collective-permute-start(bf16[128,1024]{1,0:T(8,128)(2,1)} %param.14), channel_id=1, source_target_pairs={{0,30},{2,0},{4,2},{6,4},{8,6},{10,8},{12,10},{14,12},{16,14},{18,... | collective-permute-start | bytes 786440 | tf_op jit(solution)/shard_map/ppermute | solution.py:21
  30.0 8.6 %collective-permute-start.2 = (bf16[128,1024]{1,0:T(8,128)(2,1)S(1)}, bf16[128,1024]{1,0:T(8,128)(2,1)S(1)}, u32[]{:S(2)}, u32[]{:S(2)}) collective-permute-start(bf16[128,1024]{1,0:T(8,128)(2,1)S(1)} %collective-permute-done.1), channel_id=1, source_target_pairs={{0,2},{2,4},{4,6},{6,8},{8,10},{10,12},{12,14},{14,16},{16,18},{18... | collective-permute-start | bytes 786440 | tf_op jit(solution)/shard_map/ppermute | solution.py:19
  30.2 8.5 %collective-permute-start.9 = (bf16[128,1024]{1,0:T(8,128)(2,1)S(1)}, bf16[128,1024]{1,0:T(8,128)(2,1)S(1)}, u32[]{:S(2)}, u32[]{:S(2)}) collective-permute-start(bf16[128,1024]{1,0:T(8,128)(2,1)S(1)} %collective-permute-done.8), channel_id=1, source_target_pairs={{0,30},{2,0},{4,2},{6,4},{8,6},{10,8},{12,10},{14,12},{16,14},{18,... | collective-permute-start | bytes 786440 | tf_op jit(solution)/shard_map/ppermute | solution.py:21
  38.6 8.6 %collective-permute-start.3 = (bf16[128,1024]{1,0:T(8,128)(2,1)S(1)}, bf16[128,1024]{1,0:T(8,128)(2,1)S(1)}, u32[]{:S(2)}, u32[]{:S(2)}) collective-permute-start(bf16[128,1024]{1,0:T(8,128)(2,1)S(1)} %collective-permute-done.2), channel_id=1, source_target_pairs={{0,2},{2,4},{4,6},{6,8},{8,10},{10,12},{12,14},{14,16},{16,18},{18... | collective-permute-start | bytes 786440 | tf_op jit(solution)/shard_map/ppermute | solution.py:19
  38.7 12.4 %collective-permute-start.10 = (bf16[128,1024]{1,0:T(8,128)(2,1)S(1)}, bf16[128,1024]{1,0:T(8,128)(2,1)S(1)}, u32[]{:S(2)}, u32[]{:S(2)}) collective-permute-start(bf16[128,1024]{1,0:T(8,128)(2,1)S(1)} %collective-permute-done.9), channel_id=1, source_target_pairs={{0,30},{2,0},{4,2},{6,4},{8,6},{10,8},{12,10},{14,12},{16,14},{18,... | collective-permute-start | bytes 786440 | tf_op jit(solution)/shard_map/ppermute | solution.py:21
  47.2 10.4 %collective-permute-start.4 = (bf16[128,1024]{1,0:T(8,128)(2,1)S(1)}, bf16[128,1024]{1,0:T(8,128)(2,1)S(1)}, u32[]{:S(2)}, u32[]{:S(2)}) collective-permute-start(bf16[128,1024]{1,0:T(8,128)(2,1)S(1)} %collective-permute-done.3), channel_id=1, source_target_pairs={{0,2},{2,4},{4,6},{6,8},{8,10},{10,12},{12,14},{14,16},{16,18},{18... | collective-permute-start | bytes 786440 | tf_op jit(solution)/shard_map/ppermute | solution.py:19
  51.1 8.9 %collective-permute-start.11 = (bf16[128,1024]{1,0:T(8,128)(2,1)S(1)}, bf16[128,1024]{1,0:T(8,128)(2,1)S(1)}, u32[]{:S(2)}, u32[]{:S(2)}) collective-permute-start(bf16[128,1024]{1,0:T(8,128)(2,1)S(1)} %collective-permute-done.10), channel_id=1, source_target_pairs={{0,30},{2,0},{4,2},{6,4},{8,6},{10,8},{12,10},{14,12},{16,14},{18,... | collective-permute-start | bytes 786440 | tf_op jit(solution)/shard_map/ppermute | solution.py:21
  57.6 15.0 %copy-start.3 = (bf16[128,1024]{1,0:T(8,128)(2,1)}, bf16[128,1024]{1,0:T(8,128)(2,1)S(1)}, u32[]{:S(2)}) copy-start(bf16[128,1024]{1,0:T(8,128)(2,1)S(1)} %collective-permute-done.4) | copy-start | bytes 786436
  57.6 8.6 %collective-permute-start.5 = (bf16[128,1024]{1,0:T(8,128)(2,1)S(1)}, bf16[128,1024]{1,0:T(8,128)(2,1)S(1)}, u32[]{:S(2)}, u32[]{:S(2)}) collective-permute-start(bf16[128,1024]{1,0:T(8,128)(2,1)S(1)} %collective-permute-done.4), channel_id=1, source_target_pairs={{0,2},{2,4},{4,6},{6,8},{8,10},{10,12},{12,14},{14,16},{16,18},{18... | collective-permute-start | bytes 786440 | tf_op jit(solution)/shard_map/ppermute | solution.py:19
  60.0 12.5 %collective-permute-start.12 = (bf16[128,1024]{1,0:T(8,128)(2,1)S(1)}, bf16[128,1024]{1,0:T(8,128)(2,1)}, u32[]{:S(2)}, u32[]{:S(2)}) collective-permute-start(bf16[128,1024]{1,0:T(8,128)(2,1)S(1)} %collective-permute-done.11), channel_id=1, source_target_pairs={{0,30},{2,0},{4,2},{6,4},{8,6},{10,8},{12,10},{14,12},{16,14},{18,... | collective-permute-start | bytes 786440 | tf_op jit(solution)/shard_map/ppermute | solution.py:21
  66.1 11.1 %copy-start.5 = (bf16[128,1024]{1,0:T(8,128)(2,1)}, bf16[128,1024]{1,0:T(8,128)(2,1)S(1)}, u32[]{:S(2)}) copy-start(bf16[128,1024]{1,0:T(8,128)(2,1)S(1)} %collective-permute-done.5) | copy-start | bytes 786436
  66.1 14.1 %collective-permute-start.6 = (bf16[128,1024]{1,0:T(8,128)(2,1)S(1)}, bf16[128,1024]{1,0:T(8,128)(2,1)}, u32[]{:S(2)}, u32[]{:S(2)}) collective-permute-start(bf16[128,1024]{1,0:T(8,128)(2,1)S(1)} %collective-permute-done.5), channel_id=1, source_target_pairs={{0,2},{2,4},{4,6},{6,8},{8,10},{10,12},{12,14},{14,16},{16,18},{18... | collective-permute-start | bytes 786440 | tf_op jit(solution)/shard_map/ppermute | solution.py:19
  72.5 9.1 %collective-permute-start.13 = (bf16[128,1024]{1,0:T(8,128)(2,1)}, bf16[128,1024]{1,0:T(8,128)(2,1)}, u32[]{:S(2)}, u32[]{:S(2)}) collective-permute-start(bf16[128,1024]{1,0:T(8,128)(2,1)} %collective-permute-done.12), channel_id=1, source_target_pairs={{0,30},{2,0},{4,2},{6,4},{8,6},{10,8},{12,10},{14,12},{16,14},{18,... | collective-permute-start | bytes 786440 | tf_op jit(solution)/shard_map/ppermute | solution.py:21
  80.2 9.2 %collective-permute-start.7 = (bf16[128,1024]{1,0:T(8,128)(2,1)}, bf16[128,1024]{1,0:T(8,128)(2,1)}, u32[]{:S(2)}, u32[]{:S(2)}) collective-permute-start(bf16[128,1024]{1,0:T(8,128)(2,1)} %collective-permute-done.6), channel_id=1, source_target_pairs={{0,2},{2,4},{4,6},{6,8},{8,10},{10,12},{12,14},{14,16},{16,18},{18... | collective-permute-start | bytes 786440 | tf_op jit(solution)/shard_map/ppermute | solution.py:19
  81.6 15.9 %copy-start.6 = (bf16[128,1024]{1,0:T(8,128)(2,1)S(1)}, bf16[128,1024]{1,0:T(8,128)(2,1)}, u32[]{:S(2)}) copy-start(bf16[128,1024]{1,0:T(8,128)(2,1)} %copy-done.5) | copy-start | bytes 786436
  81.6 15.9 %copy-start.4 = (bf16[128,1024]{1,0:T(8,128)(2,1)S(1)}, bf16[128,1024]{1,0:T(8,128)(2,1)}, u32[]{:S(2)}) copy-start(bf16[128,1024]{1,0:T(8,128)(2,1)} %copy-done.3) | copy-start | bytes 786436
  81.6 13.9 %collective-permute-start.14 = (bf16[128,1024]{1,0:T(8,128)(2,1)}, bf16[128,1024]{1,0:T(8,128)(2,1)S(1)}, u32[]{:S(2)}, u32[]{:S(2)}) collective-permute-start(bf16[128,1024]{1,0:T(8,128)(2,1)} %collective-permute-done.13), channel_id=1, source_target_pairs={{0,30},{2,0},{4,2},{6,4},{8,6},{10,8},{12,10},{14,12},{16,14},{18,... | collective-permute-start | bytes 786440 | tf_op jit(solution)/shard_map/ppermute | solution.py:21
  155.3 4.7 %copy-start.7 = (f32[1024]{0:T(1024)S(1)}, f32[1024]{0:T(1024)}, u32[]{:S(2)}) copy-start(f32[1024]{0:T(1024)} %param.15) | copy-start | bytes 12292
  163.4 8.4 %copy-start = (bf16[64,4,8,128]{3,2,1,0:T(8,128)(2,1)}, bf16[64,4,8,128]{3,2,1,0:T(8,128)(2,1)S(1)}, u32[]{:S(2)}) copy-start(bf16[64,4,8,128]{3,2,1,0:T(8,128)(2,1)S(1)} %reshape.187) | copy-start | bytes 1572868
  171.0 223.7 %all-gather.14.cloned.1.call-start = ((), (), s32[]{:S(2)}) async-start(), calls=%async_computation.4 | async-start | bytes 4456448 | tf_op jit(solution)/shard_map/all_gather | solution.py:124
  171.6 246.3 %reduce-scatter.2.cloned.1.call-start = ((), (), s32[]{:S(2)}) async-start(), calls=%async_computation.5 | async-start | bytes 1572864 | tf_op jit(solution)/shard_map/reduce_scatter | solution.py:126
  339.8 35.5 %copy-start.1 = (f32[64,4,8,128]{3,2,1,0:T(8,128)S(1)}, f32[64,4,8,128]{3,2,1,0:T(8,128)}, u32[]{:S(2)}) copy-start(f32[64,4,8,128]{3,2,1,0:T(8,128)} %get-tuple-element.147) | copy-start | bytes 3145732
  339.8 39.3 %copy-start.8 = (f32[1024]{0:T(1024)S(1)}, f32[1024]{0:T(1024)}, u32[]{:S(2)}) copy-start(f32[1024]{0:T(1024)} %param.16) | copy-start | bytes 12292
Sparse Core Ops, SparseCore 0:
  10.3 23.9 all-gather.7
  36.5 58.6 all-gather.11
  97.4 53.2 all-gather.9
  171.1 168.6 all-gather.15
  341.8 52.8 all-gather.13
  399.2 18.5 reduce-scatter.1
